TPU v7x, 32 devices: a whole 2x2x4 slice. The times are simulated.
32 devices in a mesh: ep: 8 (over z, x), tp: 4 (over y, core).
Axes of the slice: x: 2, y: 2, z: 4, core: 2. Of those that a mesh axis runs over, the one named last changes fastest.
Arguments:
- tokens: bfloat16 [64, 2048], P('ep'), may hold values from -6 to 6
- mix_gain: bfloat16 [2048], replicated, may hold values from 0.099609375 to 1.8984375
- w_query: bfloat16 [2048, 512], P(None, 'tp'), may hold values from -0.125 to 0.125
- w_key: bfloat16 [2048, 512], P(None, 'tp'), may hold values from -0.125 to 0.125
- w_value: bfloat16 [2048, 512], P(None, 'tp'), may hold values from -0.125 to 0.125
- w_igate: bfloat16 [2048, 4], replicated, may hold values from -0.125 to 0.125
- w_fgate: bfloat16 [2048, 4], replicated, may hold values from -0.125 to 0.125
- forget_bias: float32 [4], replicated, may hold values from 0.5 to 4.5
- w_out: bfloat16 [512, 2048], P('tp'), may hold values from -0.25 to 0.25
- mem_state: float32 [64, 4, 16384], P('ep', 'tp'), may hold values from -0.75 to 0.75
- norm_state: float32 [64, 512], P('ep', 'tp'), may hold values from -0.75 to 0.75
- max_state: float32 [64, 4], P('ep', 'tp'), may hold values from -3 to 3
- ffn_gain: bfloat16 [2048], replicated, may hold values from 0.099609375 to 1.8984375
- route_ids: int32 [64, 2], P('ep'), may hold values from 0 to 7, all different within a row; in each aligned block of 8 rows (0 to 7, 8 to 15, ...) at most 3 rows name the same one
- route_weights: float32 [64, 2], P('ep'), may hold values from 0.1 to 1
- w_gate: bfloat16 [2048, 32768], P(None, ('ep', 'tp')), may hold values from -0.125 to 0.125
- w_up: bfloat16 [2048, 32768], P(None, ('ep', 'tp')), may hold values from -0.125 to 0.125
- w_down: bfloat16 [32768, 2048], P('ep', 'tp'), may hold values from -0.09375 to 0.09375
Outputs:
- out_tokens: bfloat16 [64, 2048], P('ep', 'tp')
- new_memory: float32 [64, 4, 16384], P('ep', 'tp')
- new_norm: float32 [64, 512], P('ep', 'tp')
- new_max: float32 [64, 4], P('ep', 'tp')
Inputs may be any that keep to these rules, and one draw needn't show every extreme that they name: `route_ids`: each row names 2 different experts; among the rows of one index of ep no expert is named more than 3 times, a bound that some block reaches.
All inputs are finite; a program needn't handle non-finite values.
Results may differ from a plain program's by a relative error of at most 0.013.
The roundings to bfloat16 on the way count: a program that leaves them out, or rounds other values in their place, can miss the bound.
Values may be sent and summed in bfloat16 or wider, within the bound.
A program may use at most 64 MiB of HBM per device.

v0:
```python
import jax
import jax.numpy as jnp
from jax import lax
from jax.sharding import PartitionSpec as P

FF = 4096
epsilon = 1e-06


def scaled_rows(row_data, squares, feature_count, gain_values):
    factor = lax.rsqrt(squares / feature_count + epsilon)
    return (row_data * factor[:, None] * gain_values.astype(jnp.float32)).astype(jnp.bfloat16)


def rounded_wide(matrix):
    return lax.optimization_barrier(matrix.astype(jnp.bfloat16)).astype(jnp.float32)


def shards(
    tokens,
    mix_gain,
    w_query,
    w_key,
    w_value,
    w_igate,
    w_fgate,
    forget_bias,
    w_out,
    mem_state,
    norm_state,
    max_state,
    ffn_gain,
    route_ids,
    route_weights,
    w_gate,
    w_up,
    w_down,
):
    seq_count, model_width = tokens.shape
    local_heads = mem_state.shape[1]
    head_dim = norm_state.shape[1] // local_heads
    tp_count = lax.axis_size("tp")
    tp_at = lax.axis_index("tp")
    ep_count = lax.axis_size("ep")
    own_width = model_width // tp_count
    top_count = route_ids.shape[1]
    block_units = w_down.shape[0]
    span_count = FF // block_units
    experts = ep_count // span_count
    slot_cap = max(2, 3 * seq_count * top_count // (2 * experts))
    residual_in = tokens.astype(jnp.float32)
    normed = scaled_rows(residual_in, jnp.sum(residual_in * residual_in, 1), model_width, mix_gain)

    def project(weight):
        product = jnp.dot(normed, weight, preferred_element_type=jnp.float32)
        return rounded_wide(product).reshape(seq_count, local_heads, head_dim)

    query_rows = project(w_query)
    key_rows = project(w_key) * head_dim ** (-0.5)
    value_rows = project(w_value)
    head_start = tp_at * local_heads
    input_gate = lax.dynamic_slice_in_dim(
        jnp.dot(normed, w_igate, preferred_element_type=jnp.float32), head_start, local_heads, 1
    )
    forget_pre = jnp.dot(normed, w_fgate, preferred_element_type=jnp.float32) + forget_bias[None, :]
    forget_log = jax.nn.log_sigmoid(
        lax.dynamic_slice_in_dim(forget_pre, head_start, local_heads, 1)
    )
    new_max = jnp.maximum(forget_log + max_state, input_gate)
    keep_weight = jnp.exp(forget_log + max_state - new_max)
    new_weight = jnp.exp(input_gate - new_max)
    memory = mem_state.reshape(seq_count, local_heads, head_dim, head_dim)
    new_memory = (
        keep_weight[:, :, None, None] * memory
        + new_weight[:, :, None, None] * key_rows[:, :, :, None] * value_rows[:, :, None, :]
    )
    new_norm = (
        keep_weight[:, :, None] * norm_state.reshape(seq_count, local_heads, head_dim)
        + new_weight[:, :, None] * key_rows
    )
    numerator = jnp.einsum("shd,shde->she", query_rows, new_memory, precision=lax.Precision.HIGHEST)
    denominator = jnp.sum(query_rows * new_norm, axis=2)
    readout = (numerator / jnp.maximum(jnp.abs(denominator), jnp.exp(-new_max))[:, :, None]).astype(
        jnp.bfloat16
    )
    readout = readout.reshape(seq_count, local_heads * head_dim)
    partial_value = jnp.dot(readout, w_out, preferred_element_type=jnp.float32)
    head_total = lax.psum(partial_value.astype(jnp.bfloat16), "tp").astype(jnp.float32)
    residual = (residual_in + head_total).astype(jnp.bfloat16)
    residual_wide = lax.optimization_barrier(residual).astype(jnp.float32)
    outgoing = scaled_rows(
        residual_wide, jnp.sum(residual_wide * residual_wide, 1), model_width, ffn_gain
    )
    own_residual = lax.dynamic_slice_in_dim(residual, tp_at * own_width, own_width, 1)
    flat_ids = route_ids.reshape(-1)
    matches = (flat_ids[:, None] == jnp.arange(experts, dtype=jnp.int32)[None, :]).astype(jnp.int32)
    slot_rank = jnp.sum((jnp.cumsum(matches, 0) - matches) * matches, 1)
    slot_index = (flat_ids * slot_cap + slot_rank).reshape(seq_count, top_count)
    chosen = (
        slot_index[:, :, None] == jnp.arange(experts * slot_cap, dtype=jnp.int32)[None, None, :]
    ).astype(jnp.float32)
    placing = jnp.sum(chosen, 1).astype(jnp.bfloat16)
    mixing = jnp.sum(chosen * route_weights[:, :, None], 1)
    packed = jnp.einsum("sj,sc->jc", placing, outgoing, preferred_element_type=jnp.float32).astype(
        jnp.bfloat16
    )
    packed_width = packed.shape[1]
    outbound = jnp.broadcast_to(
        packed.reshape(experts, 1, slot_cap, packed_width),
        (experts, span_count, slot_cap, packed_width),
    ).reshape(ep_count, slot_cap, packed_width)
    arrived = lax.all_to_all(outbound, "ep", split_axis=0, concat_axis=0, tiled=True)
    sources = arrived.shape[0]
    item_count = arrived.shape[1]
    flat_rows = arrived.reshape(sources * item_count, arrived.shape[2])
    gate_sum = jnp.dot(flat_rows, w_gate, preferred_element_type=jnp.float32)
    up_sum = jnp.dot(flat_rows, w_up, preferred_element_type=jnp.float32)
    hidden = (jax.nn.silu(gate_sum) * up_sum).astype(jnp.bfloat16)
    partial_out = jnp.dot(
        lax.all_gather(hidden, "tp", axis=1, tiled=True), w_down, preferred_element_type=jnp.float32
    )
    returned = lax.all_to_all(
        partial_out.reshape(sources, item_count, w_down.shape[1]).astype(jnp.bfloat16),
        "ep",
        split_axis=0,
        concat_axis=0,
        tiled=True,
    ).astype(jnp.float32)
    results = jnp.sum(returned.reshape(experts, span_count, slot_cap, own_width), 1).reshape(
        experts * slot_cap, own_width
    )
    routed = jnp.dot(
        mixing, results, precision=lax.Precision.HIGHEST, preferred_element_type=jnp.float32
    )
    out_tokens = (own_residual.astype(jnp.float32) + routed).astype(jnp.bfloat16)
    return (
        out_tokens,
        new_memory.reshape(seq_count, local_heads, head_dim * head_dim),
        new_norm.reshape(seq_count, local_heads * head_dim),
        new_max,
    )


def solution(mesh):
    placed = (
        P("ep", None),
        P(),
        P(None, "tp"),
        P(None, "tp"),
        P(None, "tp"),
        P(),
        P(),
        P(),
        P("tp", None),
        P("ep", "tp", None),
        P("ep", "tp"),
        P("ep", "tp"),
        P(),
        P("ep", None),
        P("ep", None),
        P(None, ("ep", "tp")),
        P(None, ("ep", "tp")),
        P("ep", "tp"),
    )
    return jax.shard_map(
        shards,
        mesh=mesh,
        in_specs=placed,
        out_specs=(P("ep", "tp"), P("ep", "tp", None), P("ep", "tp"), P("ep", "tp")),
        check_vma=False,
    )
```

profile of v0, /device:TPU:0, one launch (start us, length us, event | category | flops | bytes accessed | tf_op | source)
XLA Modules:
  0.0 65.1 jit_solution(17769218186569641081)
XLA Ops:
  0.6 0.9 %fusion.9 = f32[8]{0:T(128)S(1)} fusion(bf16[8,2048]{1,0:T(8,128)(2,1)} %param.18), kind=kLoop, calls=%fused_computation.25 | loop fusion | flops 49144 | bytes 32800 | tf_op jit(solution)/shard_map/reduce_sum | solution.py:52
  1.6 0.8 %copy.36 = s32[8,2]{1,0:T(8,128)S(1)} copy(s32[8,2]{0,1:T(2,128)} %param.31) | data formatting | bytes 128 | tf_op args[13]
  2.4 0.7 %copy.34 = f32[8,1]{1,0:T(8,128)S(1)} copy(f32[8,1]{0,1:T(1,128)} %param.29) | data formatting | bytes 64 | tf_op args[11]
  3.2 0.7 %convert_element_type.78 = f32[2048]{0:T(1024)S(1)} convert(bf16[2048]{0:T(1024)(128)(2,1)} %param.19) | non-fusion elementwise | flops 2048 | bytes 12288 | tf_op jit(solution)/shard_map/convert_element_type | solution.py:12
  3.9 1.3 %convolution_convert_fusion.4 = bf16[8,128]{1,0:T(8,128)(2,1)S(1)} fusion(bf16[2048,128]{1,0:T(8,128)(2,1)} %param.21, bf16[8,2048]{1,0:T(8,128)(2,1)} %param.18, f32[2048]{0:T(1024)S(1)} %convert_element_type.78, f32[8]{0:T(128)S(1)} %add_rsqrt_fusion.1), kind=kOutput, calls=%fused_computation.9 | convolution fusion | flops 4260864 | bytes 567328 | tf_op jit(solution)/shard_map/dot_general | solution.py:55
  5.2 1.3 %convolution_convert_fusion.3 = bf16[8,128]{1,0:T(8,128)(2,1)S(1)} fusion(bf16[2048,128]{1,0:T(8,128)(2,1)} %param.22, bf16[8,2048]{1,0:T(8,128)(2,1)} %param.18, f32[2048]{0:T(1024)S(1)} %convert_element_type.78, f32[8]{0:T(128)S(1)} %add_rsqrt_fusion.1), kind=kOutput, calls=%fused_computation.8 | convolution fusion | flops 4260864 | bytes 567328 | tf_op jit(solution)/shard_map/dot_general | solution.py:55
  6.5 1.3 %convolution_convert_fusion.5 = bf16[8,128]{1,0:T(8,128)(2,1)S(1)} fusion(bf16[2048,128]{1,0:T(8,128)(2,1)} %param.20, bf16[8,2048]{1,0:T(8,128)(2,1)} %param.18, f32[2048]{0:T(1024)S(1)} %convert_element_type.78, f32[8]{0:T(128)S(1)} %add_rsqrt_fusion.1), kind=kOutput, calls=%fused_computation.10 | convolution fusion | flops 4260864 | bytes 567328 | tf_op jit(solution)/shard_map/dot_general | solution.py:55
  7.8 1.0 %fusion.24 = f32[8,4]{1,0:T(8,128)S(1)} fusion(bf16[2048,4]{0,1:T(4,128)(2,1)} %param.23, bf16[8,2048]{1,0:T(8,128)(2,1)} %param.18, f32[2048]{0:T(1024)S(1)} %convert_element_type.78, f32[8]{0:T(128)S(1)} %add_rsqrt_fusion.1), kind=kOutput, calls=%fused_computation.55 | convolution fusion | flops 196608 | bytes 57504 | tf_op jit(solution)/shard_map/dot_general | solution.py:63
  8.7 1.0 %convolution_add_fusion.1 = f32[8,4]{1,0:T(8,128)S(1)} fusion(bf16[2048,4]{0,1:T(4,128)(2,1)} %param.24, f32[4]{0:T(128)} %param.25, bf16[8,2048]{1,0:T(8,128)(2,1)} %param.18, f32[2048]{0:T(1024)S(1)} %convert_element_type.78, f32[8]{0:T(128)S(1)} %add_rsqrt_fusion.1), kind=kOutput, calls=%fused_computation.7 | convolution fusion | flops 196640 | bytes 57520 | tf_op jit(solution)/shard_map/dot_general | solution.py:65
  9.7 0.2 multiply_reduce_fusion.1
  9.9 1.5 %multiply_reduce_fusion = (f32[8]{0:T(128)S(1)}, f32[8,128]{1,0:T(8,128)}, f32[8,128]{1,0:T(8,128)S(1)}) fusion(bf16[8,128]{1,0:T(8,128)(2,1)S(1)} %convolution_convert_fusion.5, f32[8]{0:T(128)S(1)} %get-tuple-element.16, bf16[8,128]{1,0:T(8,128)(2,1)S(1)} %convolution_convert_fusion.4, f32[8,128]{1,0:T(8,128)} %param.28, f32[8]{0:T(128)S(1)} %get-tuple-element.17), kind=kLoop, calls=%fused_computation.44 | loop fusion | flops 7160 | bytes 16480 | tf_op jit(solution)/shard_map/reduce_sum | solution.py:82
  12.0 0.7 %convert_element_type.95 = f32[2048]{0:T(1024)S(1)} convert(bf16[2048]{0:T(1024)(128)(2,1)} %param.30) | non-fusion elementwise | flops 2048 | bytes 12288 | tf_op jit(solution)/shard_map/convert_element_type | solution.py:12
  12.8 1.5 %fusion.2 = f32[8,1,128]{2,1,0:T(1,128)S(1)} fusion(f32[8,128,128]{2,1,0:T(8,128)} %bitcast.22, f32[8]{0:T(128)S(1)} %get-tuple-element.17, f32[8,128]{1,0:T(8,128)S(1)} %convert_element_type.84, f32[8,128]{1,0:T(8,128)S(1)} %get-tuple-element.23, bf16[8,128,1]{1,0,2:T(8,128)(2,1)S(1)} %bitcast.24), kind=kOutput, calls=%fused_computation.12 | convolution fusion | flops 1966080 | bytes 538656 | tf_op jit(solution)/shard_map/shd,shde->she/dot_general | solution.py:81
  14.3 0.2 convolution_convert_fusion.1
  14.5 12.9 %psum.7 = bf16[8,2048]{1,0:T(8,128)(2,1)S(1)} all-reduce(bf16[8,2048]{1,0:T(8,128)(2,1)S(1)} %convolution_convert_fusion.1), channel_id=1, replica_groups=mesh['ep'=8,'tp'=4] {'tp'}, use_global_device_ids=true, to_apply=%region_2.3 | all-reduce | flops 16384 | bytes 65536 | tf_op jit(solution)/shard_map/psum | solution.py:88
  27.5 0.8 %fusion.12 = bf16[8,2048]{1,0:T(8,128)(2,1)S(1)} fusion(bf16[8,2048]{1,0:T(8,128)(2,1)} %param.18, bf16[8,2048]{1,0:T(8,128)(2,1)S(1)} %psum.7), kind=kLoop, calls=%fused_computation.28 | loop fusion | flops 65536 | bytes 98304 | tf_op jit(solution)/shard_map/convert_element_type | solution.py:89
  28.4 0.8 %convert_reduce_fusion = (bf16[8,24]{1,0:T(8,128)(2,1)S(1)}, f32[8,24]{1,0:T(8,128)S(1)}) fusion(s32[8,2]{0,1:T(2,128)S(1)} %copy.38, f32[8,2]{0,1:T(2,128)} %param.32), kind=kLoop, calls=%fused_computation.32 | loop fusion | flops 1536 | bytes 1280 | tf_op jit(solution)/shard_map/reduce_sum | solution.py:102
  29.2 0.2 convolution_convert_fusion
  29.4 0.7 %reshape_reshape.3 = bf16[8,3,2048]{2,1,0:T(4,128)(2,1)} reshape(bf16[24,2048]{1,0:T(8,128)(2,1)S(1)} %convolution_convert_fusion) | data formatting | bytes 196608 | tf_op jit(solution)/shard_map/reshape;reshape | solution.py:111
  30.1 5.8 %all-to-all-start = ((bf16[8,3,2048]{2,1,0:T(4,128)(2,1)}), bf16[8,3,2048]{2,1,0:T(4,128)(2,1)S(1)}, u32[]{:S(2)}, u32[]{:S(2)}) async-start(bf16[8,3,2048]{2,1,0:T(4,128)(2,1)} %reshape_reshape.3), calls=%async_computation | async-start | bytes 262144 | tf_op jit(solution)/shard_map/all_to_all | solution.py:112
  36.1 7.1 %all-to-all-done = bf16[8,3,2048]{2,1,0:T(4,128)(2,1)S(1)} async-done(((bf16[8,3,2048]{2,1,0:T(4,128)(2,1)}), bf16[8,3,2048]{2,1,0:T(4,128)(2,1)S(1)}, u32[]{:S(2)}, u32[]{:S(2)}) %all-to-all-start) | async-done | bytes 98336 | tf_op jit(solution)/shard_map/all_to_all | solution.py:112
  43.4 3.0 %fusion.28 = f32[24,1024]{1,0:T(8,128)S(1)} fusion(bf16[24,2048]{1,0:T(8,128)(2,1)S(1)} %reshape.138, bf16[2048,1024]{1,0:T(8,128)(2,1)} %param.33), kind=kOutput, calls=%fused_computation.56 | convolution fusion | flops 100663296 | bytes 4390912 | tf_op jit(solution)/shard_map/dot_general | solution.py:116
  46.4 0.4 copy-done.1
  46.8 0.7 %fusion = bf16[24,1024]{1,0:T(8,128)(2,1)S(1)} fusion(bf16[24,2048]{1,0:T(8,128)(2,1)S(1)} %reshape.138, bf16[2048,1024]{1,0:T(8,128)(2,1)S(1)} %copy-done.1, f32[24,1024]{1,0:T(8,128)S(1)} %fusion.28), kind=kOutput, calls=%fused_computation.3 | convolution fusion | flops 100810752 | bytes 4440064 | tf_op jit(solution)/shard_map/dot_general | solution.py:117
  47.5 5.6 %all_gather.3 = bf16[24,4096]{1,0:T(8,128)(2,1)S(1)} all-gather(bf16[24,1024]{1,0:T(8,128)(2,1)S(1)} %fusion), channel_id=1, replica_groups=mesh['ep'=8,'tp'=4] {'tp'}, dimensions={1}, use_global_device_ids=true | all-gather | bytes 245760 | tf_op jit(solution)/shard_map/all_gather | solution.py:120
  53.1 0.7 %convolution_convert_fusion.2 = bf16[24,512]{1,0:T(8,128)(2,1)S(1)} fusion(bf16[24,4096]{1,0:T(8,128)(2,1)S(1)} %all_gather.3, bf16[4096,512]{1,0:T(8,128)(2,1)S(1)} %copy-done.2), kind=kOutput, calls=%fused_computation.4 | convolution fusion | flops 100675584 | bytes 4415488 | tf_op jit(solution)/shard_map/dot_general | solution.py:119
  53.7 0.6 convert_element_type.100
  54.4 3.3 %all-to-all-start.1 = ((bf16[8,3,512]{2,1,0:T(4,128)(2,1)}), bf16[8,3,512]{2,1,0:T(4,128)(2,1)S(1)}, u32[]{:S(2)}, u32[]{:S(2)}) async-start(bf16[8,3,512]{2,1,0:T(4,128)(2,1)} %convert_element_type.100), calls=%async_computation.1 | async-start | bytes 65536 | tf_op jit(solution)/shard_map/all_to_all | solution.py:122
  57.7 1.4 %multiply_add_fusion = f32[8,1,16384]{2,1,0:T(1,128)} fusion(f32[8,1,16384]{2,1,0:T(1,128)S(1)} %bitcast.23, f32[8,1,16384]{2,1,0:T(1,128)S(1)} %copy-done.3, f32[8]{0:T(128)S(1)} %get-tuple-element.17), kind=kLoop, calls=%fused_computation.11 | loop fusion | flops 262144 | bytes 1572896 | tf_op jit(solution)/shard_map/add | solution.py:74
  59.1 0.6 copy.39
  59.7 4.6 %all-to-all-done.1 = bf16[8,3,512]{2,1,0:T(4,128)(2,1)S(1)} async-done(((bf16[8,3,512]{2,1,0:T(4,128)(2,1)}), bf16[8,3,512]{2,1,0:T(4,128)(2,1)S(1)}, u32[]{:S(2)}, u32[]{:S(2)}) %all-to-all-start.1) | async-done | bytes 24608 | tf_op jit(solution)/shard_map/all_to_all | solution.py:122
  64.4 0.7 %fusion.1 = bf16[8,512]{1,0:T(8,128)(2,1)} fusion(f32[8,24]{1,0:T(8,128)S(1)} %get-tuple-element.19, bf16[24,512]{1,0:T(8,128)(2,1)S(1)} %reshape.139, bf16[8,2048]{1,0:T(8,128)(2,1)S(1)} %fusion.12, s32[]{:T(128)S(6)} %select_n.14), kind=kOutput, calls=%fused_computation.6 | convolution fusion | flops 1191936 | bytes 41732 | tf_op jit(solution)/shard_map/dot_general | solution.py:132
  (24 shorter events, 1.2 us)
Async XLA Ops:
  0.6 13.7 %copy-start = (bf16[128,2048]{1,0:T(8,128)(2,1)S(1)}, bf16[128,2048]{1,0:T(8,128)(2,1)}, u32[]{:S(2)}) copy-start(bf16[128,2048]{1,0:T(8,128)(2,1)} %param.26) | copy-start | bytes 1572868
  30.1 13.1 %all-to-all-start = ((bf16[8,3,2048]{2,1,0:T(4,128)(2,1)}), bf16[8,3,2048]{2,1,0:T(4,128)(2,1)S(1)}, u32[]{:S(2)}, u32[]{:S(2)}) async-start(bf16[8,3,2048]{2,1,0:T(4,128)(2,1)} %reshape_reshape.3), calls=%async_computation | async-start | bytes 262144 | tf_op jit(solution)/shard_map/all_to_all | solution.py:112
  43.4 3.5 %copy-start.1 = (bf16[2048,1024]{1,0:T(8,128)(2,1)S(1)}, bf16[2048,1024]{1,0:T(8,128)(2,1)}, u32[]{:S(2)}) copy-start(bf16[2048,1024]{1,0:T(8,128)(2,1)} %param.34) | copy-start | bytes 12582916
  43.4 9.7 %copy-start.2 = (bf16[4096,512]{1,0:T(8,128)(2,1)S(1)}, bf16[4096,512]{1,0:T(8,128)(2,1)}, u32[]{:S(2)}) copy-start(bf16[4096,512]{1,0:T(8,128)(2,1)} %param.35) | copy-start | bytes 12582916
  46.8 10.9 %copy-start.3 = (f32[8,1,16384]{2,1,0:T(1,128)S(1)}, f32[8,1,16384]{2,1,0:T(1,128)}, u32[]{:S(2)}) copy-start(f32[8,1,16384]{2,1,0:T(1,128)} %param.27) | copy-start | bytes 1572868
  54.4 10.0 %all-to-all-start.1 = ((bf16[8,3,512]{2,1,0:T(4,128)(2,1)}), bf16[8,3,512]{2,1,0:T(4,128)(2,1)S(1)}, u32[]{:S(2)}, u32[]{:S(2)}) async-start(bf16[8,3,512]{2,1,0:T(4,128)(2,1)} %convert_element_type.100), calls=%async_computation.1 | async-start | bytes 65536 | tf_op jit(solution)/shard_map/all_to_all | solution.py:122
where the time goes:
time: 65.9 us; the launch traced here: 65.1 us
  blocking collectives  18.5 us (28%)
  matrix products  12.9 us (20%)
  waiting for transfers between devices  11.8 us (18%)
  starting transfers between devices  9.14 us (14%)
  other arithmetic  7.75 us (12%)
  local copies, waits for them, and re-layouts  4.36 us (7%)
  between operations  0.72 us (1%)
    psum x1, blocking collectives, shards(): lax.psum(partial_value.astype(jnp.bfloat16), 'tp').astype(jnp.float32)  12.9 us
    all_to_all x1, waiting for transfers between devices, shards(): lax.all_to_all(outbound, 'ep', split_axis=0, concat_axis=0, tiled=True)  7.14 us
    all_to_all x1, starting transfers between devices, shards(): lax.all_to_all(outbound, 'ep', split_axis=0, concat_axis=0, tiled=True)  5.8 us
    all_gather x1, blocking collectives, shards(): lax.all_gather(hidden, 'tp', axis=1, tiled=True)  5.59 us
    all_to_all x1, waiting for transfers between devices, shards(): lax.all_to_all(partial_out.reshape(sources, item_count, w_down.shape[1])....  4.63 us
    dot_general x3, matrix products, project(): product = jnp.dot(normed, weight, preferred_element_type=jnp.float32)  3.89 us
    all_to_all x1, starting transfers between devices, shards(): lax.all_to_all(partial_out.reshape(sources, item_count, w_down.shape[1])....  3.33 us
    dot_general x1, matrix products, shards(): gate_sum = jnp.dot(flat_rows, w_gate, preferred_element_type=jnp.float32)  2.99 us
  transfers between devices with their start and end apart: 2, of which 2 were waited for; matrix products, arithmetic and copies ran while one was open for 3% of the time, Pallas kernels for 0%

commit v1 on v0

--- a/solution.py
+++ b/solution.py
@@ -117,7 +117,9 @@
     up_sum = jnp.dot(flat_rows, w_up, preferred_element_type=jnp.float32)
     hidden = (jax.nn.silu(gate_sum) * up_sum).astype(jnp.bfloat16)
     partial_out = jnp.dot(
-        lax.all_gather(hidden, "tp", axis=1, tiled=True), w_down, preferred_element_type=jnp.float32
+        jnp.concatenate(lax.all_gather(hidden, "tp"), axis=1),
+        w_down,
+        preferred_element_type=jnp.float32,
     )
     returned = lax.all_to_all(
         partial_out.reshape(sources, item_count, w_down.shape[1]).astype(jnp.bfloat16),

time: 65.9 us -> 68.6 us (1.041)
  matrix products: 12.9 us -> 15 us
    dot_general x1, matrix products: 0.65 us -> 2.84 us  [shards(): jnp.dot(jnp.concatenate(lax.all_gather(hidden, 'tp'), axis=1), w_down, pr...]
    unnamed x11 -> x9, local copies, waits for them, and re-layouts: 2.53 us -> 2.54 us
where the time goes in v1:
time: 68.6 us; the launch traced here: 67.8 us
  blocking collectives  18.7 us (27%)
  matrix products  15 us (22%)
  waiting for transfers between devices  11.8 us (17%)
  starting transfers between devices  9.14 us (13%)
  other arithmetic  7.75 us (11%)
  local copies, waits for them, and re-layouts  4.67 us (7%)
  between operations  0.73 us (1%)
    psum x1, blocking collectives, shards(): lax.psum(partial_value.astype(jnp.bfloat16), 'tp').astype(jnp.float32)  12.9 us
    all_to_all x1, waiting for transfers between devices, shards(): lax.all_to_all(outbound, 'ep', split_axis=0, concat_axis=0, tiled=True)  7.14 us
    all_to_all x1, starting transfers between devices, shards(): lax.all_to_all(outbound, 'ep', split_axis=0, concat_axis=0, tiled=True)  5.81 us
    all_gather x1, blocking collectives, shards(): lax.all_gather(hidden, 'tp')  5.73 us
    all_to_all x1, waiting for transfers between devices, shards(): lax.all_to_all(partial_out.reshape(sources, item_count, w_down.shape[1])....  4.63 us
    dot_general x3, matrix products, project(): product = jnp.dot(normed, weight, preferred_element_type=jnp.float32)  3.89 us
    all_to_all x1, starting transfers between devices, shards(): lax.all_to_all(partial_out.reshape(sources, item_count, w_down.shape[1])....  3.33 us
    dot_general x1, matrix products, shards(): gate_sum = jnp.dot(flat_rows, w_gate, preferred_element_type=jnp.float32)  2.99 us
  transfers between devices with their start and end apart: 2, of which 2 were waited for; matrix products, arithmetic and copies ran while one was open for 3% of the time, Pallas kernels for 0%

profile of v1, /device:TPU:0, one launch (start us, length us, event | category | flops | bytes accessed | tf_op | source)
XLA Modules:
  0.0 67.8 jit_solution(8777585695989681386)
XLA Ops:
  0.6 0.9 %fusion.15 = f32[8]{0:T(128)S(1)} fusion(bf16[8,2048]{1,0:T(8,128)(2,1)} %param.18), kind=kLoop, calls=%fused_computation.29 | loop fusion | flops 49144 | bytes 32800 | tf_op jit(solution)/shard_map/reduce_sum | solution.py:52
  1.6 0.8 %copy.48 = s32[8,2]{1,0:T(8,128)S(1)} copy(s32[8,2]{0,1:T(2,128)} %param.31) | data formatting | bytes 128 | tf_op args[13]
  2.4 0.7 %copy.46 = f32[8,1]{1,0:T(8,128)S(1)} copy(f32[8,1]{0,1:T(1,128)} %param.29) | data formatting | bytes 64 | tf_op args[11]
  3.2 0.7 %convert_element_type.75 = f32[2048]{0:T(1024)S(1)} convert(bf16[2048]{0:T(1024)(128)(2,1)} %param.19) | non-fusion elementwise | flops 2048 | bytes 12288 | tf_op jit(solution)/shard_map/convert_element_type | solution.py:12
  3.9 1.3 %convolution_convert_fusion.3 = bf16[8,128]{1,0:T(8,128)(2,1)S(1)} fusion(bf16[2048,128]{1,0:T(8,128)(2,1)} %param.21, bf16[8,2048]{1,0:T(8,128)(2,1)} %param.18, f32[2048]{0:T(1024)S(1)} %convert_element_type.75, f32[8]{0:T(128)S(1)} %add_rsqrt_fusion.1), kind=kOutput, calls=%fused_computation.11 | convolution fusion | flops 4260864 | bytes 567328 | tf_op jit(solution)/shard_map/dot_general | solution.py:55
  5.2 1.3 %convolution_convert_fusion.2 = bf16[8,128]{1,0:T(8,128)(2,1)S(1)} fusion(bf16[2048,128]{1,0:T(8,128)(2,1)} %param.22, bf16[8,2048]{1,0:T(8,128)(2,1)} %param.18, f32[2048]{0:T(1024)S(1)} %convert_element_type.75, f32[8]{0:T(128)S(1)} %add_rsqrt_fusion.1), kind=kOutput, calls=%fused_computation.10 | convolution fusion | flops 4260864 | bytes 567328 | tf_op jit(solution)/shard_map/dot_general | solution.py:55
  6.5 1.3 %convolution_convert_fusion.4 = bf16[8,128]{1,0:T(8,128)(2,1)S(1)} fusion(bf16[2048,128]{1,0:T(8,128)(2,1)} %param.20, bf16[8,2048]{1,0:T(8,128)(2,1)} %param.18, f32[2048]{0:T(1024)S(1)} %convert_element_type.75, f32[8]{0:T(128)S(1)} %add_rsqrt_fusion.1), kind=kOutput, calls=%fused_computation.12 | convolution fusion | flops 4260864 | bytes 567328 | tf_op jit(solution)/shard_map/dot_general | solution.py:55
  7.8 1.0 %fusion.30 = f32[8,4]{1,0:T(8,128)S(1)} fusion(bf16[2048,4]{0,1:T(4,128)(2,1)} %param.23, bf16[8,2048]{1,0:T(8,128)(2,1)} %param.18, f32[2048]{0:T(1024)S(1)} %convert_element_type.75, f32[8]{0:T(128)S(1)} %add_rsqrt_fusion.1), kind=kOutput, calls=%fused_computation.59 | convolution fusion | flops 196608 | bytes 57504 | tf_op jit(solution)/shard_map/dot_general | solution.py:63
  8.7 1.0 %convolution_add_fusion.1 = f32[8,4]{1,0:T(8,128)S(1)} fusion(bf16[2048,4]{0,1:T(4,128)(2,1)} %param.24, f32[4]{0:T(128)} %param.25, bf16[8,2048]{1,0:T(8,128)(2,1)} %param.18, f32[2048]{0:T(1024)S(1)} %convert_element_type.75, f32[8]{0:T(128)S(1)} %add_rsqrt_fusion.1), kind=kOutput, calls=%fused_computation.9 | convolution fusion | flops 196640 | bytes 57520 | tf_op jit(solution)/shard_map/dot_general | solution.py:65
  9.7 0.2 multiply_reduce_fusion.1
  9.9 1.5 %multiply_reduce_fusion = (f32[8]{0:T(128)S(1)}, f32[8,128]{1,0:T(8,128)}, f32[8,128]{1,0:T(8,128)S(1)}) fusion(bf16[8,128]{1,0:T(8,128)(2,1)S(1)} %convolution_convert_fusion.4, f32[8]{0:T(128)S(1)} %get-tuple-element.20, bf16[8,128]{1,0:T(8,128)(2,1)S(1)} %convolution_convert_fusion.3, f32[8,128]{1,0:T(8,128)} %param.28, f32[8]{0:T(128)S(1)} %get-tuple-element.21), kind=kLoop, calls=%fused_computation.48 | loop fusion | flops 7160 | bytes 16480 | tf_op jit(solution)/shard_map/reduce_sum | solution.py:82
  12.0 0.7 %convert_element_type.92 = f32[2048]{0:T(1024)S(1)} convert(bf16[2048]{0:T(1024)(128)(2,1)} %param.30) | non-fusion elementwise | flops 2048 | bytes 12288 | tf_op jit(solution)/shard_map/convert_element_type | solution.py:12
  12.8 1.5 %fusion.7 = f32[8,1,128]{2,1,0:T(1,128)S(1)} fusion(f32[8,128,128]{2,1,0:T(8,128)} %bitcast.29, f32[8]{0:T(128)S(1)} %get-tuple-element.21, f32[8,128]{1,0:T(8,128)S(1)} %convert_element_type.81, f32[8,128]{1,0:T(8,128)S(1)} %get-tuple-element.27, bf16[8,128,1]{1,0,2:T(8,128)(2,1)S(1)} %bitcast.33), kind=kOutput, calls=%fused_computation.14 | convolution fusion | flops 1966080 | bytes 538656 | tf_op jit(solution)/shard_map/shd,shde->she/dot_general | solution.py:81
  14.3 0.2 convolution_convert_fusion.1
  14.5 12.9 %psum.7 = bf16[8,2048]{1,0:T(8,128)(2,1)S(1)} all-reduce(bf16[8,2048]{1,0:T(8,128)(2,1)S(1)} %convolution_convert_fusion.1), channel_id=1, replica_groups=mesh['ep'=8,'tp'=4] {'tp'}, use_global_device_ids=true, to_apply=%region_2.3 | all-reduce | flops 16384 | bytes 65536 | tf_op jit(solution)/shard_map/psum | solution.py:88
  27.5 0.8 %fusion.18 = bf16[8,2048]{1,0:T(8,128)(2,1)S(1)} fusion(bf16[8,2048]{1,0:T(8,128)(2,1)} %param.18, bf16[8,2048]{1,0:T(8,128)(2,1)S(1)} %psum.7), kind=kLoop, calls=%fused_computation.32 | loop fusion | flops 65536 | bytes 98304 | tf_op jit(solution)/shard_map/convert_element_type | solution.py:89
  28.4 0.8 %convert_reduce_fusion = (bf16[8,24]{1,0:T(8,128)(2,1)S(1)}, f32[8,24]{1,0:T(8,128)S(1)}) fusion(s32[8,2]{0,1:T(2,128)S(1)} %copy.50, f32[8,2]{0,1:T(2,128)} %param.32), kind=kLoop, calls=%fused_computation.36 | loop fusion | flops 1536 | bytes 1280 | tf_op jit(solution)/shard_map/reduce_sum | solution.py:102
  29.2 0.2 convolution_convert_fusion
  29.4 0.7 %reshape_reshape.3 = bf16[8,3,2048]{2,1,0:T(4,128)(2,1)} reshape(bf16[24,2048]{1,0:T(8,128)(2,1)S(1)} %convolution_convert_fusion) | data formatting | bytes 196608 | tf_op jit(solution)/shard_map/reshape;reshape | solution.py:111
  30.1 5.8 %all-to-all-start = ((bf16[8,3,2048]{2,1,0:T(4,128)(2,1)}), bf16[8,3,2048]{2,1,0:T(4,128)(2,1)S(1)}, u32[]{:S(2)}, u32[]{:S(2)}) async-start(bf16[8,3,2048]{2,1,0:T(4,128)(2,1)} %reshape_reshape.3), calls=%async_computation | async-start | bytes 262144 | tf_op jit(solution)/shard_map/all_to_all | solution.py:112
  36.1 7.1 %all-to-all-done = bf16[8,3,2048]{2,1,0:T(4,128)(2,1)S(1)} async-done(((bf16[8,3,2048]{2,1,0:T(4,128)(2,1)}), bf16[8,3,2048]{2,1,0:T(4,128)(2,1)S(1)}, u32[]{:S(2)}, u32[]{:S(2)}) %all-to-all-start) | async-done | bytes 98336 | tf_op jit(solution)/shard_map/all_to_all | solution.py:112
  43.4 3.0 %fusion.34 = f32[24,1024]{1,0:T(8,128)S(1)} fusion(bf16[24,2048]{1,0:T(8,128)(2,1)S(1)} %reshape.143, bf16[2048,1024]{1,0:T(8,128)(2,1)} %param.33), kind=kOutput, calls=%fused_computation.60 | convolution fusion | flops 100663296 | bytes 4390912 | tf_op jit(solution)/shard_map/dot_general | solution.py:116
  46.4 0.4 copy-done.1
  46.8 0.7 fusion.2
  47.5 5.7 %all-gather = bf16[96,1024]{1,0:T(8,128)(2,1)S(1)} all-gather(bf16[24,1024]{1,0:T(8,128)(2,1)S(1)} %fusion.2), channel_id=2, replica_groups=mesh['ep'=8,'tp'=4] {'tp'}, dimensions={0}, use_global_device_ids=true | all-gather | bytes 245760 | tf_op jit(solution)/shard_map/all_gather | solution.py:120
  53.6 2.8 %fusion.3 = bf16[8,3,512]{2,0,1:T(8,128)(2,1)S(1)} fusion(bf16[4096,512]{1,0:T(8,128)(2,1)} %param.35, bf16[8,3,4096]{2,1,0:T(4,128)(2,1)S(1)} %dot_general.48), kind=kOutput, calls=%fused_computation.6 | convolution fusion | flops 100675584 | bytes 4415488 | tf_op jit(solution)/shard_map/dot_general | solution.py:119
  56.4 0.6 copy.53
  57.0 3.3 %all-to-all-start.1 = ((bf16[8,3,512]{2,1,0:T(4,128)(2,1)}), bf16[8,3,512]{2,1,0:T(4,128)(2,1)S(1)}, u32[]{:S(2)}, u32[]{:S(2)}) async-start(bf16[8,3,512]{2,1,0:T(4,128)(2,1)} %copy.53), calls=%async_computation.1 | async-start | bytes 65536 | tf_op jit(solution)/shard_map/all_to_all | solution.py:124
  60.4 1.4 %multiply_add_fusion = f32[8,1,16384]{2,1,0:T(1,128)} fusion(f32[8,1,16384]{2,1,0:T(1,128)S(1)} %bitcast.30, f32[8,1,16384]{2,1,0:T(1,128)S(1)} %copy-done.2, f32[8]{0:T(128)S(1)} %get-tuple-element.21), kind=kLoop, calls=%fused_computation.13 | loop fusion | flops 262144 | bytes 1572896 | tf_op jit(solution)/shard_map/add | solution.py:74
  61.8 0.6 copy.54
  62.4 4.6 %all-to-all-done.1 = bf16[8,3,512]{2,1,0:T(4,128)(2,1)S(1)} async-done(((bf16[8,3,512]{2,1,0:T(4,128)(2,1)}), bf16[8,3,512]{2,1,0:T(4,128)(2,1)S(1)}, u32[]{:S(2)}, u32[]{:S(2)}) %all-to-all-start.1) | async-done | bytes 24608 | tf_op jit(solution)/shard_map/all_to_all | solution.py:124
  67.0 0.7 %fusion.6 = bf16[8,512]{1,0:T(8,128)(2,1)} fusion(f32[8,24]{1,0:T(8,128)S(1)} %get-tuple-element.23, bf16[24,512]{1,0:T(8,128)(2,1)S(1)} %reshape.145, bf16[8,2048]{1,0:T(8,128)(2,1)S(1)} %fusion.18, s32[]{:T(128)S(6)} %select_n.14), kind=kOutput, calls=%fused_computation.8 | convolution fusion | flops 1191936 | bytes 41732 | tf_op jit(solution)/shard_map/dot_general | solution.py:134
  (24 shorter events, 1.6 us)
Async XLA Ops:
  0.6 13.7 %copy-start = (bf16[128,2048]{1,0:T(8,128)(2,1)S(1)}, bf16[128,2048]{1,0:T(8,128)(2,1)}, u32[]{:S(2)}) copy-start(bf16[128,2048]{1,0:T(8,128)(2,1)} %param.26) | copy-start | bytes 1572868
  30.1 13.1 %all-to-all-start = ((bf16[8,3,2048]{2,1,0:T(4,128)(2,1)}), bf16[8,3,2048]{2,1,0:T(4,128)(2,1)S(1)}, u32[]{:S(2)}, u32[]{:S(2)}) async-start(bf16[8,3,2048]{2,1,0:T(4,128)(2,1)} %reshape_reshape.3), calls=%async_computation | async-start | bytes 262144 | tf_op jit(solution)/shard_map/all_to_all | solution.py:112
  43.4 3.5 %copy-start.1 = (bf16[2048,1024]{1,0:T(8,128)(2,1)S(1)}, bf16[2048,1024]{1,0:T(8,128)(2,1)}, u32[]{:S(2)}) copy-start(bf16[2048,1024]{1,0:T(8,128)(2,1)} %param.34) | copy-start | bytes 12582916
  47.5 12.9 %copy-start.2 = (f32[8,1,16384]{2,1,0:T(1,128)S(1)}, f32[8,1,16384]{2,1,0:T(1,128)}, u32[]{:S(2)}) copy-start(f32[8,1,16384]{2,1,0:T(1,128)} %param.27) | copy-start | bytes 1572868
  57.0 10.0 %all-to-all-start.1 = ((bf16[8,3,512]{2,1,0:T(4,128)(2,1)}), bf16[8,3,512]{2,1,0:T(4,128)(2,1)S(1)}, u32[]{:S(2)}, u32[]{:S(2)}) async-start(bf16[8,3,512]{2,1,0:T(4,128)(2,1)} %copy.53), calls=%async_computation.1 | async-start | bytes 65536 | tf_op jit(solution)/shard_map/all_to_all | solution.py:124
